TPU v7x, 512 devices: a 4x2x32 block of a 4x8x32 slice. The times are simulated.
512 devices in a mesh: grp: 2 (over y), ep: 64 (over z, core), tp: 4 (over x).
Axes of the slice: x: 4, y: 2, z: 32, core: 2. Of those that a mesh axis runs over, the one named last changes fastest.
The devices are a block of a 4x8x32 slice.
Arguments:
- tokens: bfloat16 [49152, 2048], P(('grp', 'ep'), 'tp'), parts along dimension 0
- group_choice: int32 [49152], P(('grp', 'ep')), parts along dimension 0, may hold values from 0 to 7, as said below
- expert_choice: int32 [49152, 2], P(('grp', 'ep')), parts along dimension 0, may hold values from 0 to 7, as said below
- group_weight: float32 [49152], P(('grp', 'ep')), parts along dimension 0, may hold values from 0.3 to 1
- expert_weight: float32 [49152, 2], P(('grp', 'ep')), parts along dimension 0, may hold values from 0.1 to 1
- norm_gain: float32 [2048], replicated, may hold values from 0.1 to 1.9
- w_gate: bfloat16 [64, 2048, 1024], P('ep', None, 'tp'), may hold values from -0.125 to 0.125
- w_up: bfloat16 [64, 2048, 1024], P('ep', None, 'tp'), may hold values from -0.125 to 0.125
- w_down: bfloat16 [64, 1024, 2048], P('ep', None, 'tp'), may hold values from -0.1875 to 0.1875
Outputs:
- moe_out: bfloat16 [49152, 2048], P(('grp', 'ep'), 'tp'), parts along dimension 0
There are 2 independent parts, one for each index of `grp`. A program takes and returns all parts, laid end to end along the dimension named above; an argument that names none is the same for every part. Nothing has to cross between parts.
Inputs may be any that keep to these rules, and one draw needn't show every extreme that they name: `group_choice`: group of each token, 0 to 7; within each aligned block of 384 tokens (the tokens of one index of ep) every group is chosen by the same number of tokens. `expert_choice`: a token's two entries differ; within each aligned block of 384 tokens no expert (group with entry) is named by more than 18 tokens, and in every block one expert of each group, the same one in all blocks, is named by exactly 18 tokens.
All inputs are finite; a program needn't handle non-finite values.
Results may differ from a plain program's by a relative error of at most 0.0071.
Values may be sent and summed in bfloat16 or wider, within the bound.
A program may use at most 64 MiB of HBM per device.

v0:
```python
import jax
import jax.numpy as jnp
from jax import lax
from jax.sharding import Mesh
from jax.sharding import PartitionSpec as P

EP = ("ep_0", "ep_1")
GRP_EP = ("grp", "ep_0", "ep_1")


def copy_for_each(array, axis):
    length = lax.axis_size(axis)
    return lax.all_to_all(
        jnp.broadcast_to(array[None], (length, *array.shape)), axis, 0, 0, tiled=True
    )


def laid_out(blocks, dim):
    dims = list(blocks.shape[1:])
    dims[dim] *= blocks.shape[0]
    return jnp.moveaxis(blocks, 0, dim).reshape(dims)


def collect(array, axis, dim):
    blocks = copy_for_each(array, axis)
    return laid_out(blocks, dim)


def over_copies(array, axis):
    everything = copy_for_each(array, axis)
    return jnp.sum(everything, axis=0)


def cut_along(array, dim, length):
    dims = array.shape
    blocks = array.reshape(*dims[:dim], length, dims[dim] // length, *dims[dim + 1 :])
    return jnp.moveaxis(blocks, dim, 0)


def moved_by_axis(blocks, axes, turns):
    dims = [lax.axis_size(a) for a in axes]
    blocks = blocks.reshape(*dims, *blocks.shape[1:])
    for k in turns:
        blocks = lax.all_to_all(blocks, axes[k], split_axis=k, concat_axis=k, tiled=True)
    return blocks.reshape(-1, *blocks.shape[len(axes) :])


def exchange_by_chip(array, groups, turns, split_dim, concat_dim):
    length = lax.axis_size(groups[0]) * lax.axis_size(groups[1])
    blocks = cut_along(array, split_dim, length)
    return laid_out(moved_by_axis(blocks, groups, turns), concat_dim)


def finish_rows(gate_sum, up_sum, w_down):
    hidden = (jax.nn.silu(gate_sum) * up_sum).astype(jnp.bfloat16)
    whole_hidden = collect(hidden, "tp", 3)
    summed = jnp.einsum("sxcf,xfd->sxcd", whole_hidden, w_down, preferred_element_type=jnp.float32)
    return summed.astype(jnp.bfloat16)


def body(
    tokens,
    group_choice,
    expert_choice,
    group_weight,
    expert_weight,
    norm_gain,
    w_gate,
    w_up,
    w_down,
):
    tok_rows = tokens.shape[0]
    ep_count = lax.axis_size(EP)
    exp_local = w_gate.shape[0]
    experts_all = ep_count * exp_local
    group_size = min(8, experts_all // 2)
    group_count = experts_all // group_size
    mean_load = 2 * tok_rows // experts_all
    capacity = mean_load + min(mean_load // 2, tok_rows // group_count - mean_load)
    model_width = norm_gain.shape[0]
    expert_ids = group_choice[:, None] * group_size + expert_choice
    mixing = group_weight[:, None] * expert_weight / jnp.sum(expert_weight, -1, keepdims=True)
    flat_ids = expert_ids.reshape(-1)
    marks = (flat_ids[:, None] == jnp.arange(experts_all, dtype=jnp.int32)[None, :]).astype(
        jnp.int32
    )
    earlier = jnp.cumsum(marks, 0) - marks
    seat_index = jnp.sum(earlier * marks, 1)
    targets = (flat_ids * capacity + seat_index).reshape(tok_rows, 2)
    places = jnp.arange(experts_all * capacity, dtype=jnp.int32)
    dispatch = (
        (places[:, None] == targets[None, :, 0]) | (places[:, None] == targets[None, :, 1])
    ).astype(jnp.bfloat16)
    values = tokens.astype(jnp.float32)
    own_squares = jnp.sum(values * values, -1)
    all_squares = over_copies(own_squares, "tp")
    inv_rms = lax.rsqrt(all_squares / model_width + 1e-06)
    piece_width = tokens.shape[1]
    gain_piece = lax.dynamic_slice_in_dim(
        norm_gain, lax.axis_index("tp") * piece_width, piece_width, 0
    )
    normed = (values * inv_rms[:, None] * gain_piece[None, :]).astype(jnp.bfloat16)
    buffer = jnp.dot(dispatch, normed, preferred_element_type=jnp.float32).astype(jnp.bfloat16)
    buffer = buffer.reshape(ep_count, exp_local, capacity, piece_width)
    piece = lax.all_gather(
        lax.all_to_all(buffer, EP, split_axis=0, concat_axis=0, tiled=True),
        "tp",
        axis=3,
        tiled=True,
    )
    gate_next = jnp.einsum("sxcd,xdf->sxcf", piece, w_gate, preferred_element_type=jnp.float32)
    up_next = jnp.einsum("sxcd,xdf->sxcf", piece, w_up, preferred_element_type=jnp.float32)
    results = finish_rows(gate_next, up_next, w_down)
    returned = exchange_by_chip(results, ("ep_0", "ep_1"), (1, 0), 0, 0)
    returned = returned.reshape(experts_all * capacity, returned.shape[3])
    combined = jnp.zeros((tok_rows, returned.shape[1]), jnp.float32)
    for choice_index in range(2):
        picker = (targets[:, choice_index : choice_index + 1] == places[None, :]).astype(
            jnp.bfloat16
        )
        picked = jnp.dot(picker, returned, preferred_element_type=jnp.float32)
        combined = combined + mixing[:, choice_index : choice_index + 1] * picked
    return combined.astype(jnp.bfloat16)


def solution(mesh):
    split = Mesh(
        mesh.devices.reshape(mesh.shape["grp"], 32, 2, mesh.shape["tp"]),
        ("grp", "ep_0", "ep_1", "tp"),
    )
    placed = (
        P(GRP_EP, "tp"),
        P(GRP_EP),
        P(GRP_EP, None),
        P(GRP_EP),
        P(GRP_EP, None),
        P(),
        P(EP, None, "tp"),
        P(EP, None, "tp"),
        P(EP, None, "tp"),
    )
    return jax.shard_map(
        body, mesh=split, in_specs=placed, out_specs=P(GRP_EP, "tp"), check_vma=False
    )
```

profile of v0, /device:TPU:41, one launch (start us, length us, event | category | flops | bytes accessed | tf_op | source)
XLA Modules:
  0.0 481.0 jit_solution(356377158643691526)
XLA Ops:
  6.6 1.2 fusion.35
  8.4 4.3 all-to-all-start
  12.7 0.8 copy.35
  14.7 1.8 reduce-window.6
  17.5 0.8 dynamic_slice.3
  18.3 1.9 convolution_convert_fusion
  20.2 2.2 reshape.67
  22.3 199.5 %all_to_all.26 = bf16[64,1,18,512]{3,2,1,0:T(8,128)(2,1)S(1)} all-to-all(bf16[64,1,18,512]{3,2,1,0:T(8,128)(2,1)S(1)} %bitcast.87), channel_id=1, replica_groups=mesh['grp'=2,'ep_0'=32,'ep_1'=2,'tp'=4] {'ep_0','ep_1'}, dimensions={0} | all-to-all | bytes 2359296 | tf_op jit(solution)/shard_map/all_to_all | solution.py:106
  221.9 1.4 copy.39
  223.4 52.3 %all-gather.2.cloned.1.call-done = bf16[64,1,18,2048]{3,0,2,1:T(8,128)(2,1)} async-done(((bf16[64,1,18,512]{3,0,2,1:T(8,128)(2,1)}), bf16[64,1,18,2048]{3,0,2,1:T(8,128)(2,1)}) %all-gather.2.cloned.1.call-update) | async-done | bytes 4718608 | tf_op jit(solution)/shard_map/all_gather | solution.py:105
  275.7 3.9 fusion.9
  279.6 1.5 fusion.25
  281.4 31.1 %all_to_all.27 = bf16[4,64,1,18,256]{4,1,3,2,0:T(8,128)(2,1)S(1)} all-to-all(bf16[4,64,1,18,256]{4,1,3,2,0:T(8,128)(2,1)S(1)} %broadcast_in_dim.8), channel_id=1, replica_groups=mesh['grp'=2,'ep_0'=32,'ep_1'=2,'tp'=4] {'tp'}, dimensions={0} | all-to-all | bytes 4718592 | tf_op jit(solution)/shard_map/all_to_all | solution.py:13
  312.4 2.0 copy.40
  314.5 2.9 reshape.71
  317.4 3.0 fusion.8
  321.2 6.3 %all_to_all.28 = bf16[32,2,1,1,18,512]{5,0,4,3,2,1:T(8,128)(2,1)S(1)} all-to-all(bf16[32,2,1,1,18,512]{5,0,4,3,2,1:T(8,128)(2,1)S(1)} %copy.41), channel_id=1, replica_groups=mesh['grp'=2,'ep_0'=32,'ep_1'=2,'tp'=4] {'ep_1'}, dimensions={1} | all-to-all | bytes 2359296 | tf_op jit(solution)/shard_map/all_to_all | solution.py:44
  327.5 2.3 copy.42
  329.8 23.4 %all-to-all-start.4 = ((bf16[32,2,1,1,18,512]{5,1,4,3,2,0:T(2,128)(2,1)}), bf16[32,2,1,1,18,512]{5,1,4,3,2,0:T(2,128)(2,1)}, u32[]{:S(2)}, u32[]{:S(2)}) async-start(bf16[32,2,1,1,18,512]{5,1,4,3,2,0:T(2,128)(2,1)} %copy.42), calls=%async_computation.4 | async-start | bytes 2359296 | tf_op jit(solution)/shard_map/all_to_all | solution.py:44
  353.2 114.5 %all-to-all-done.4 = bf16[32,2,1,1,18,512]{5,1,4,3,2,0:T(2,128)(2,1)} async-done(((bf16[32,2,1,1,18,512]{5,1,4,3,2,0:T(2,128)(2,1)}), bf16[32,2,1,1,18,512]{5,1,4,3,2,0:T(2,128)(2,1)}, u32[]{:S(2)}, u32[]{:S(2)}) %all-to-all-start.4) | async-done | bytes 1179680 | tf_op jit(solution)/shard_map/all_to_all | solution.py:44
  467.7 1.6 copy.43
  469.3 1.2 reshape_reshape_reshape.3
  470.5 2.1 fusion.23
  472.6 1.5 fusion.24
  (39 shorter events, 3.9 us)
Async XLA Ops:
  6.5 310.9 %copy-start = (bf16[1,1024,512]{2,1,0:T(8,128)(2,1)S(1)}, bf16[1,1024,512]{2,1,0:T(8,128)(2,1)}, u32[]{:S(2)}) copy-start(bf16[1,1024,512]{2,1,0:T(8,128)(2,1)} %param.17) | copy-start | bytes 3145732
  8.4 9.8 %all-to-all-start = ((f32[4,1,384]{2,1,0:T(1,128)}), f32[4,1,384]{2,1,0:T(1,128)S(1)}, u32[]{:S(2)}, u32[]{:S(2)}) async-start(f32[4,1,384]{2,1,0:T(1,128)} %broadcast_in_dim.6), calls=%async_computation | async-start | bytes 12288 | tf_op jit(solution)/shard_map/all_to_all | solution.py:13
  12.7 263.0 %all-gather.2.cloned.1.call-start = ((), (), s32[]{:S(2)}) async-start(), calls=%async_computation.5 | async-start | bytes 5898240 | tf_op jit(solution)/shard_map/all_gather | solution.py:105
  14.5 3.8 copy-start.2
  223.3 52.4 %copy-start.6 = (bf16[1,2048,256]{2,1,0:T(8,128)(2,1)S(1)}, bf16[1,2048,256]{2,1,0:T(8,128)(2,1)}, u32[]{:S(2)}) copy-start(bf16[1,2048,256]{2,1,0:T(8,128)(2,1)} %param.15) | copy-start | bytes 3145732
  223.3 56.2 %copy-start.7 = (bf16[1,2048,256]{2,1,0:T(8,128)(2,1)S(1)}, bf16[1,2048,256]{2,1,0:T(8,128)(2,1)}, u32[]{:S(2)}) copy-start(bf16[1,2048,256]{2,1,0:T(8,128)(2,1)} %param.16) | copy-start | bytes 3145732
  275.7 3.9 copy-start.5
  329.8 23.4 %copy-start.3 = (f32[384,2]{0,1:T(2,128)S(1)}, f32[384,2]{0,1:T(2,128)}, u32[]{:S(2)}) copy-start(f32[384,2]{0,1:T(2,128)} %param.13) | copy-start | bytes 9220
  329.8 23.4 %copy-start.4 = (f32[384]{0:T(512)S(1)}, f32[384]{0:T(512)}, u32[]{:S(2)}) copy-start(f32[384]{0:T(512)} %param.12) | copy-start | bytes 4612
  329.8 137.9 %all-to-all-start.4 = ((bf16[32,2,1,1,18,512]{5,1,4,3,2,0:T(2,128)(2,1)}), bf16[32,2,1,1,18,512]{5,1,4,3,2,0:T(2,128)(2,1)}, u32[]{:S(2)}, u32[]{:S(2)}) async-start(bf16[32,2,1,1,18,512]{5,1,4,3,2,0:T(2,128)(2,1)} %copy.42), calls=%async_computation.4 | async-start | bytes 2359296 | tf_op jit(solution)/shard_map/all_to_all | solution.py:44
  470.5 2.1 copy-start.1
Sparse Core Ops, SparseCore 0:
  223.5 52.1 all-gather.1
where the time goes:
time: 483 us; the launch traced here: 481 us
  blocking collectives  237 us (49%)
  waiting for transfers between devices  167 us (35%)
  starting transfers between devices  27.7 us (6%)
  local copies, waits for them, and re-layouts  17.8 us (4%)
  matrix products  13.8 us (3%)
  between operations  13.6 us (3%)
    all_to_all x1, blocking collectives, body(): lax.all_to_all(buffer, EP, split_axis=0, concat_axis=0, tiled=True)  200 us
    all_to_all x1, waiting for transfers between devices, moved_by_axis(): lax.all_to_all(blocks, axes[k], split_axis=k, concat_axis=k, tiled=True)  115 us
    all_gather x1, waiting for transfers between devices, body(): lax.all_gather(lax.all_to_all(buffer, EP, split_axis=0, concat_axis=0, ti...  52.3 us
    all_to_all x1, blocking collectives, copy_for_each(): lax.all_to_all(jnp.broadcast_to(array[None], (length, *array.shape)), axi...  31.1 us
    all_to_all x1, starting transfers between devices, moved_by_axis(): lax.all_to_all(blocks, axes[k], split_axis=k, concat_axis=k, tiled=True)  23.4 us
  transfers between devices with their start and end apart: 3, of which 2 were waited for; matrix products, arithmetic and copies ran while one was open for 1% of the time, Pallas kernels for 0%

commit v1 on v0

v1 whole, which is shorter than its diff:
```python
import jax
import jax.numpy as jnp
from jax import lax
from jax.sharding import Mesh
from jax.sharding import PartitionSpec as P

GRP_EP = ("grp", "g", "e")
EP = ("g", "e")
GROUP_SIZE = 8


def rank_before(marks):
    return jnp.cumsum(marks, -2) - marks


def body(
    tokens,
    group_choice,
    expert_choice,
    group_weight,
    expert_weight,
    norm_gain,
    w_gate,
    w_up,
    w_down,
):
    rows, width = tokens.shape
    groups = lax.axis_size("g")
    members = lax.axis_size("e")
    per_group = rows // groups
    mean_load = 2 * per_group // members
    capacity = mean_load + min(mean_load // 2, per_group - mean_load)
    model_width = norm_gain.shape[0]
    mixing = group_weight[:, None] * expert_weight / jnp.sum(expert_weight, -1, keepdims=True)

    group_marks = (group_choice[:, None] == jnp.arange(groups, dtype=jnp.int32)).astype(jnp.int32)
    place = group_choice * per_group + jnp.sum(rank_before(group_marks) * group_marks, 1)
    spots = jnp.arange(rows, dtype=jnp.int32)
    sort = spots[:, None] == place[None, :]

    values = tokens.astype(jnp.float32)
    squares = lax.all_gather(jnp.sum(values * values, -1), "tp", axis=0)
    inv_rms = lax.rsqrt(jnp.sum(squares, 0) / model_width + 1e-06)
    gain = lax.dynamic_slice_in_dim(norm_gain, lax.axis_index("tp") * width, width, 0)
    normed = (values * inv_rms[:, None] * gain[None, :]).astype(jnp.bfloat16)
    by_group = jnp.dot(
        sort.astype(jnp.bfloat16), normed, preferred_element_type=jnp.float32
    ).astype(jnp.bfloat16)
    facts = jnp.concatenate([expert_choice.astype(jnp.float32), mixing], -1)
    facts = jnp.dot(sort.astype(jnp.float32), facts, precision=lax.Precision.HIGHEST)
    landed = lax.all_to_all(
        by_group.reshape(groups, per_group, width), "g", 0, 0, tiled=True
    ).reshape(rows, width)
    facts = lax.all_to_all(
        facts.reshape(groups, per_group, 4), "g", 0, 0, tiled=True
    ).reshape(rows, 4)

    chosen = facts[:, :2].astype(jnp.int32).reshape(groups, per_group, 2)
    blocks = jnp.arange(groups, dtype=jnp.int32)[:, None, None]
    kinds = jnp.arange(members, dtype=jnp.int32)
    marks = jnp.sum((chosen[..., None] == kinds).astype(jnp.int32), 2)
    ranks = rank_before(marks)
    seats = jnp.sum(
        jnp.where(chosen[..., None] == kinds, ranks[:, :, None, :], 0), -1
    )
    targets = (chosen * groups + blocks) * capacity + seats
    targets = targets.reshape(rows, 2)
    seats_all = members * groups * capacity
    places = jnp.arange(seats_all, dtype=jnp.int32)
    picks = [targets[None, :, k] == places[:, None] for k in range(2)]
    dispatch = (picks[0] | picks[1]).astype(jnp.bfloat16)
    buffer = jnp.dot(dispatch, landed, preferred_element_type=jnp.float32).astype(jnp.bfloat16)
    received = lax.all_to_all(
        buffer.reshape(members, groups * capacity, width), "e", 0, 0, tiled=True
    ).reshape(seats_all, width)

    piece = lax.all_gather(received, "tp", axis=1, tiled=True)
    gate = jnp.dot(piece, w_gate[0], preferred_element_type=jnp.float32)
    up = jnp.dot(piece, w_up[0], preferred_element_type=jnp.float32)
    hidden = (jax.nn.silu(gate) * up).astype(jnp.bfloat16)
    hidden = lax.all_gather(hidden, "tp", axis=1, tiled=True)
    result = jnp.dot(hidden, w_down[0], preferred_element_type=jnp.float32).astype(jnp.bfloat16)
    back = lax.all_to_all(
        result.reshape(members, groups * capacity, width), "e", 0, 0, tiled=True
    ).reshape(seats_all, width)

    mixed = jnp.zeros((rows, width), jnp.float32)
    for k in range(2):
        picker = (targets[:, k : k + 1] == places[None, :]).astype(jnp.bfloat16)
        picked = jnp.dot(picker, back, preferred_element_type=jnp.float32)
        mixed = mixed + facts[:, 2 + k : 3 + k] * picked
    home = lax.all_to_all(
        mixed.astype(jnp.bfloat16).reshape(groups, per_group, width), "g", 0, 0, tiled=True
    ).reshape(rows, width)
    unsort = place[:, None] == spots[None, :]
    return jnp.dot(
        unsort.astype(jnp.bfloat16), home, preferred_element_type=jnp.float32
    ).astype(jnp.bfloat16)


def solution(mesh):
    members = GROUP_SIZE
    split = Mesh(
        mesh.devices.reshape(
            mesh.shape["grp"], mesh.shape["ep"] // members, members, mesh.shape["tp"]
        ),
        ("grp", "g", "e", "tp"),
    )
    placed = (
        P(GRP_EP, "tp"),
        P(GRP_EP),
        P(GRP_EP, None),
        P(GRP_EP),
        P(GRP_EP, None),
        P(),
        P(EP, None, "tp"),
        P(EP, None, "tp"),
        P(EP, None, "tp"),
    )
    return jax.shard_map(
        body, mesh=split, in_specs=placed, out_specs=P(GRP_EP, "tp"), check_vma=False
    )
```

time: 483 us -> 405 us (0.84); the launches traced: 481 us -> 398 us
  blocking collectives: 237 us -> 125 us
  starting transfers between devices: 27.7 us -> 63.2 us
  local copies, waits for them, and re-layouts: 17.8 us -> 3.1 us
  other arithmetic: 4.2 us -> 11 us
    all_to_all x3 -> x2, blocking collectives: 237 us -> 116 us  [the longest x1 62.9 us: body(): lax.all_to_all(mixed.astype(jnp.bfloat16).reshape(groups, per_group, widt...]
    all_to_all x2 -> x3, waiting for transfers between devices: 115 us -> 63 us  [the longest x1 28.4 us: body(): lax.all_to_all(result.reshape(members, groups * capacity, width), 'e', 0,...]
    all_gather x1 -> x2, waiting for transfers between devices: 52.3 us -> 103 us  [the longest x1 51.9 us: body(): hidden = lax.all_gather(hidden, 'tp', axis=1, tiled=True)]
    all_to_all x2 -> x3, starting transfers between devices: 27.7 us -> 63.1 us  [the longest x1 43.2 us: body(): lax.all_to_all(facts.reshape(groups, per_group, 4), 'g', 0, 0, tiled=True)]
    all_gather x0 -> x1, blocking collectives: none -> 8.79 us  [body(): squares = lax.all_gather(jnp.sum(values * values, -1), 'tp', axis=0)]
    another operation x4 -> x0, local copies, waits for them, and re-layouts: 4.84 us -> none
    dot_general x6 -> x9, matrix products: 13.8 us -> 16.3 us  [the longest x1 4.07 us: body(): jnp.dot(hidden, w_down[0], preferred_element_type=jnp.float32)]
  transfers between devices with their start and end apart: 3 -> 5, of which waited for: 2 -> 5; matrix products, arithmetic and copies ran while one was open for 1% -> 3% of each run, Pallas kernels for 0% -> 0%
where the time goes in v1:
time: 405 us; the launch traced here: 398 us
  waiting for transfers between devices  166 us (41%)
  blocking collectives  125 us (31%)
  starting transfers between devices  63.2 us (16%)
  matrix products  16.3 us (4%)
  between operations  13.6 us (3%)
  other arithmetic  11 us (3%)
    all_to_all x1, blocking collectives, body(): lax.all_to_all(mixed.astype(jnp.bfloat16).reshape(groups, per_group, widt...  62.9 us
    all_to_all x1, blocking collectives, body(): lax.all_to_all(buffer.reshape(members, groups * capacity, width), 'e', 0,...  53.5 us
    all_gather x1, waiting for transfers between devices, body(): hidden = lax.all_gather(hidden, 'tp', axis=1, tiled=True)  51.9 us
    all_gather x1, waiting for transfers between devices, body(): piece = lax.all_gather(received, 'tp', axis=1, tiled=True)  50.7 us
    all_to_all x1, starting transfers between devices, body(): lax.all_to_all(facts.reshape(groups, per_group, 4), 'g', 0, 0, tiled=True)  43.2 us
    all_to_all x1, waiting for transfers between devices, body(): lax.all_to_all(result.reshape(members, groups * capacity, width), 'e', 0,...  28.4 us
    all_to_all x1, waiting for transfers between devices, body(): lax.all_to_all(by_group.reshape(groups, per_group, width), 'g', 0, 0, til...  26.6 us
    all_to_all x1, starting transfers between devices, body(): lax.all_to_all(by_group.reshape(groups, per_group, width), 'g', 0, 0, til...  13.1 us
  transfers between devices with their start and end apart: 5, of which 5 were waited for; matrix products, arithmetic and copies ran while one was open for 3% of the time, Pallas kernels for 0%

profile of v1, /device:TPU:41, one launch (start us, length us, event | category | flops | bytes accessed | tf_op | source)
XLA Modules:
  0.0 398.1 jit_solution(10690738187043938088)
XLA Ops:
  6.6 0.8 convert_element_type.48
  8.0 0.8 reduce-window.6
  9.1 0.8 fusion.28
  13.2 43.2 %all-to-all-start = ((f32[8,1,192]{2,1,0:T(1,128)}), f32[8,1,192]{2,1,0:T(1,128)S(1)}, u32[]{:S(2)}, u32[]{:S(2)}) async-start(f32[8,1,192]{2,1,0:T(1,128)} %reshape.92), calls=%async_computation | async-start | bytes 16384 | tf_op jit(solution)/shard_map/all_to_all | solution.py:54
  56.3 1.2 fusion.17
  57.5 8.8 %all-gather.1 = f32[4,1,384]{2,1,0:T(1,128)S(1)} all-gather(f32[1,1,384]{2,1,0:T(1,128)S(1)} %reshape.84), channel_id=2, replica_groups=mesh['grp'=2,'g'=8,'e'=8,'tp'=4] {'tp'}, dimensions={0}, use_global_device_ids=true | all-gather | bytes 7680 | tf_op jit(solution)/shard_map/all_gather | solution.py:42
  66.3 0.8 dynamic_slice.3
  67.1 2.2 convolution_convert_fusion.3
  69.3 8.0 %all-to-all-done = f32[8,1,192]{2,1,0:T(1,128)S(1)} async-done(((f32[8,1,192]{2,1,0:T(1,128)}), f32[8,1,192]{2,1,0:T(1,128)S(1)}, u32[]{:S(2)}, u32[]{:S(2)}) %all-to-all-start) | async-done | bytes 6176 | tf_op jit(solution)/shard_map/all_to_all | solution.py:54
  77.3 13.1 %all-to-all-start.1 = ((bf16[8,48,512]{2,1,0:T(8,128)(2,1)}), bf16[8,48,512]{2,1,0:T(8,128)(2,1)S(1)}, u32[]{:S(2)}, u32[]{:S(2)}) async-start(bf16[8,48,512]{2,1,0:T(8,128)(2,1)} %bitcast.3), calls=%async_computation.1 | async-start | bytes 786432 | tf_op jit(solution)/shard_map/all_to_all | solution.py:51
  92.3 3.8 reduce-window_subtract_fusion
  96.4 26.6 %all-to-all-done.1 = bf16[8,48,512]{2,1,0:T(8,128)(2,1)S(1)} async-done(((bf16[8,48,512]{2,1,0:T(8,128)(2,1)}), bf16[8,48,512]{2,1,0:T(8,128)(2,1)S(1)}, u32[]{:S(2)}, u32[]{:S(2)}) %all-to-all-start.1) | async-done | bytes 393248 | tf_op jit(solution)/shard_map/all_to_all | solution.py:51
  122.9 0.8 convolution_convert_fusion.1
  123.7 53.5 %all_to_all.25 = bf16[8,144,512]{2,1,0:T(8,128)(2,1)} all-to-all(bf16[8,144,512]{2,1,0:T(8,128)(2,1)S(1)} %bitcast.50), channel_id=1, replica_groups=mesh['grp'=2,'g'=8,'e'=8,'tp'=4] {'e'}, dimensions={0} | all-to-all | bytes 2359296 | tf_op jit(solution)/shard_map/all_to_all | solution.py:73
  177.3 50.7 %all-gather.5.cloned.1.call-done = bf16[1152,2048]{1,0:T(8,128)(2,1)} async-done(((bf16[1152,512]{1,0:T(8,128)(2,1)}), bf16[1152,2048]{1,0:T(8,128)(2,1)}) %all-gather.5.cloned.1.call-update) | async-done | bytes 4718608 | tf_op jit(solution)/shard_map/all_gather | solution.py:77
  228.0 3.9 fusion.11
  232.0 2.4 fusion
  234.4 51.9 %all-gather.7.cloned.1.call-done = bf16[1152,1024]{1,0:T(8,128)(2,1)} async-done(((bf16[1152,256]{1,0:T(8,128)(2,1)}), bf16[1152,1024]{1,0:T(8,128)(2,1)}) %all-gather.7.cloned.1.call-update) | async-done | bytes 2359312 | tf_op jit(solution)/shard_map/all_gather | solution.py:81
  286.4 4.1 %convolution_convert_fusion = bf16[1152,512]{1,0:T(8,128)(2,1)} fusion(bf16[1152,1024]{1,0:T(8,128)(2,1)} %all-gather.7.cloned.1.call-done, bf16[1,1024,512]{2,1,0:T(8,128)(2,1)S(1)} %copy-done), kind=kOutput, calls=%fused_computation | convolution fusion | flops 1208549376 | bytes 4587520 | tf_op jit(solution)/shard_map/dot_general | solution.py:82
  290.4 6.8 %all-to-all-start.3 = ((bf16[8,144,512]{2,1,0:T(8,128)(2,1)}), bf16[8,144,512]{2,1,0:T(8,128)(2,1)S(1)}, u32[]{:S(2)}, u32[]{:S(2)}) async-start(bf16[8,144,512]{2,1,0:T(8,128)(2,1)} %bitcast.10), calls=%async_computation.3 | async-start | bytes 2359296 | tf_op jit(solution)/shard_map/all_to_all | solution.py:83
  297.3 28.4 %all-to-all-done.3 = bf16[8,144,512]{2,1,0:T(8,128)(2,1)S(1)} async-done(((bf16[8,144,512]{2,1,0:T(8,128)(2,1)}), bf16[8,144,512]{2,1,0:T(8,128)(2,1)S(1)}, u32[]{:S(2)}, u32[]{:S(2)}) %all-to-all-start.3) | async-done | bytes 1179680 | tf_op jit(solution)/shard_map/all_to_all | solution.py:83
  326.4 0.7 fusion.8
  327.1 62.9 %all_to_all.26 = bf16[8,48,512]{2,1,0:T(8,128)(2,1)S(1)} all-to-all(bf16[8,48,512]{2,1,0:T(8,128)(2,1)S(1)} %bitcast.52), channel_id=1, replica_groups=mesh['grp'=2,'g'=8,'e'=8,'tp'=4] {'g'}, dimensions={0} | all-to-all | bytes 786432 | tf_op jit(solution)/shard_map/all_to_all | solution.py:92
  390.0 1.2 convolution_convert_fusion.2
  (45 shorter events, 7.3 us)
Async XLA Ops:
  6.5 279.8 %copy-start = (bf16[1,1024,512]{2,1,0:T(8,128)(2,1)S(1)}, bf16[1,1024,512]{2,1,0:T(8,128)(2,1)}, u32[]{:S(2)}) copy-start(bf16[1,1024,512]{2,1,0:T(8,128)(2,1)} %param.17) | copy-start | bytes 3145732
  13.2 64.2 %all-to-all-start = ((f32[8,1,192]{2,1,0:T(1,128)}), f32[8,1,192]{2,1,0:T(1,128)S(1)}, u32[]{:S(2)}, u32[]{:S(2)}) async-start(f32[8,1,192]{2,1,0:T(1,128)} %reshape.92), calls=%async_computation | async-start | bytes 16384 | tf_op jit(solution)/shard_map/all_to_all | solution.py:54
  77.3 45.6 %all-to-all-start.1 = ((bf16[8,48,512]{2,1,0:T(8,128)(2,1)}), bf16[8,48,512]{2,1,0:T(8,128)(2,1)S(1)}, u32[]{:S(2)}, u32[]{:S(2)}) async-start(bf16[8,48,512]{2,1,0:T(8,128)(2,1)} %bitcast.3), calls=%async_computation.1 | async-start | bytes 786432 | tf_op jit(solution)/shard_map/all_to_all | solution.py:51
  90.4 137.6 %all-gather.5.cloned.1.call-start = ((), (), s32[]{:S(2)}) async-start(), calls=%async_computation.5 | async-start | bytes 5898240 | tf_op jit(solution)/shard_map/all_gather | solution.py:77
  177.2 50.8 %copy-start.2 = (bf16[1,2048,256]{2,1,0:T(8,128)(2,1)S(1)}, bf16[1,2048,256]{2,1,0:T(8,128)(2,1)}, u32[]{:S(2)}) copy-start(bf16[1,2048,256]{2,1,0:T(8,128)(2,1)} %param.15) | copy-start | bytes 3145732
  177.3 54.7 %copy-start.3 = (bf16[1,2048,256]{2,1,0:T(8,128)(2,1)S(1)}, bf16[1,2048,256]{2,1,0:T(8,128)(2,1)}, u32[]{:S(2)}) copy-start(bf16[1,2048,256]{2,1,0:T(8,128)(2,1)} %param.16) | copy-start | bytes 3145732
  177.3 109.1 %all-gather.7.cloned.1.call-start = ((), (), s32[]{:S(2)}) async-start(), calls=%async_computation.6 | async-start | bytes 2949120 | tf_op jit(solution)/shard_map/all_gather | solution.py:81
  228.0 3.9 copy-start.1
  290.4 35.2 %all-to-all-start.3 = ((bf16[8,144,512]{2,1,0:T(8,128)(2,1)}), bf16[8,144,512]{2,1,0:T(8,128)(2,1)S(1)}, u32[]{:S(2)}, u32[]{:S(2)}) async-start(bf16[8,144,512]{2,1,0:T(8,128)(2,1)} %bitcast.10), calls=%async_computation.3 | async-start | bytes 2359296 | tf_op jit(solution)/shard_map/all_to_all | solution.py:83
Sparse Core Ops, SparseCore 0:
  177.4 50.6 all-gather.4
  234.5 51.7 all-gather.6

commit v2 on v1

v2 whole, which is shorter than its diff:
```python
import functools

import jax
import jax.numpy as jnp
from jax import lax
from jax.experimental import pallas as pl
from jax.experimental.pallas import tpu as pltpu
from jax.sharding import Mesh
from jax.sharding import PartitionSpec as P

GRP_EP = ("grp", "g", "e")
EP = ("g", "e")
GROUP_SIZE = 8
MESH = pl.DeviceIdType.MESH
F32 = jnp.float32
BF16 = jnp.bfloat16


def dot(a, b):
    return jnp.dot(a, b, preferred_element_type=F32)


def iota(shape, dim):
    return lax.broadcasted_iota(jnp.int32, shape, dim)


def pieces(x, count):
    parts = []
    for _ in range(count):
        part = x.astype(BF16)
        parts.append(part)
        x = x - part.astype(F32)
    return parts


def remote(src, dst, send, recv, **where):
    return pltpu.make_async_remote_copy(
        src_ref=src, dst_ref=dst, send_sem=send, recv_sem=recv,
        device_id=where, device_id_type=MESH,
    )


def kernel(
    groups, members, ways, per_group, cap,
    tok, grow, gcol, crow, gw, ew, gain, wg_hbm, wu_hbm, wd_hbm,
    out,
    wg, wu, wd, sq, sorted_rows, facts, landed, facts_in, normed, rows_t, cols_t,
    picked, x, h, result, back, total, mixed, home,
    w_sem, q_send, q_recv, s1_send, s1_recv, m_send, m_recv, s2_send, s2_recv,
    x_send, x_recv, h_send, h_recv, r_send, r_recv, f_send, f_recv,
):
    my_g, my_e, my_t = lax.axis_index("g"), lax.axis_index("e"), lax.axis_index("tp")
    right, left = lax.rem(my_t + 1, ways), lax.rem(my_t + ways - 1, ways)
    across = lax.rem(my_t + 2, ways)
    rows, width = tok.shape
    chunk = groups * cap
    ff = wg.shape[1]
    lanes = 128

    loads = [
        pltpu.make_async_copy(src, dst, w_sem.at[n])
        for n, (src, dst) in enumerate(((wg_hbm, wg), (wu_hbm, wu), (wd_hbm, wd)))
    ]
    for load in loads:
        load.start()

    barrier = pltpu.get_barrier_semaphore()
    for off in range(1, groups):
        pl.semaphore_signal(
            barrier, inc=1, device_id={"g": lax.rem(my_g + off, groups)}, device_id_type=MESH
        )
    for off in range(1, members):
        pl.semaphore_signal(
            barrier, inc=1, device_id={"e": lax.rem(my_e + off, members)}, device_id_type=MESH
        )
    for off in range(1, ways):
        pl.semaphore_signal(
            barrier, inc=1, device_id={"tp": lax.rem(my_t + off, ways)}, device_id_type=MESH
        )

    earlier = iota((rows, rows), 0) < iota((rows, rows), 1)
    marks = (grow[...] == iota((groups, rows), 0)).astype(F32)
    rank_row = jnp.sum(dot(marks.astype(BF16), earlier.astype(BF16)) * marks, 0, keepdims=True)
    place_row = grow[...] * per_group + rank_row.astype(jnp.int32)
    sort = (iota((rows, rows), 0) == place_row).astype(BF16)
    sorted_rows[...] = dot(sort, tok[...]).astype(BF16).reshape(groups, per_group, width)
    values = tok[...].astype(F32)
    squares = jnp.sum(values * values, -1, keepdims=True)
    squares = jnp.transpose(jnp.broadcast_to(squares, (rows, lanes)))
    sq[my_t] = squares[:8]

    pl.semaphore_wait(barrier, groups + members + ways - 3)

    order = sorted(range(1, groups), key=lambda off: -min(off, groups - off))
    s1 = []
    q1 = []
    for off in range(1, ways):
        to = lax.rem(my_t + off, ways)
        q1.append(remote(sq.at[my_t], sq.at[my_t], q_send.at[to], q_recv.at[my_t], tp=to))
        q1[-1].start()
    for off in order:
        to = lax.rem(my_g + off, groups)
        s1.append(
            remote(sorted_rows.at[to], landed.at[my_g], s1_send.at[to], s1_recv.at[my_g], g=to)
        )
        s1[-1].start()
    landed[my_g] = sorted_rows[my_g]

    marks_c = (gcol[...] == iota((rows, groups), 1)).astype(F32)
    later = iota((rows, rows), 0) > iota((rows, rows), 1)
    rank_col = jnp.sum(dot(later.astype(BF16), marks_c.astype(BF16)) * marks_c, 1, keepdims=True)
    place_wide = gcol[...] * lanes + rank_col.astype(jnp.int32)
    spread = (iota((rows, groups * lanes), 1) == place_wide).astype(BF16)

    for off in range(1, ways):
        src = lax.rem(my_t + off, ways)
        remote(sq.at[src], sq.at[src], q_send.at[src], q_recv.at[src], tp=src).wait_recv()
    model_width = width * ways
    all_squares = jnp.sum(sq[...], 0)[:1]
    inv_rms = lax.rsqrt(all_squares / model_width + 1e-06)
    weights = ew[...]
    mixing = gw[...] * weights / jnp.sum(weights, 0, keepdims=True)
    choice = crow[...].astype(F32)
    fields = [choice[0:1], choice[1:2]]
    for k in range(2):
        fields += [p.astype(F32) for p in pieces(mixing[k : k + 1], 2)]
    fields += [p.astype(F32) for p in pieces(inv_rms, 3)]
    fields.append(jnp.zeros((16 - len(fields), rows), F32))
    fields = jnp.concatenate(fields, 0).astype(BF16)
    spread_fields = dot(fields, spread).astype(BF16)
    for n in range(groups):
        facts[n] = spread_fields[:, n * lanes : (n + 1) * lanes]
    m1 = []
    for off in order:
        to = lax.rem(my_g + off, groups)
        m1.append(remote(facts.at[to], facts_in.at[my_g], m_send.at[to], m_recv.at[my_g], g=to))
        m1[-1].start()
    facts_in[my_g] = facts[my_g]

    def block_of(shape, dim):
        spot = iota(shape, dim)
        block = jnp.zeros(shape, jnp.int32)
        for n in range(1, groups):
            block = block + (spot >= n * per_group).astype(jnp.int32)
        return block

    for off in order:
        src = lax.rem(my_g + off, groups)
        remote(facts.at[src], facts_in.at[src], m_send.at[src], m_recv.at[src], g=src).wait_recv()
    known = jnp.zeros((16, rows), F32)
    for n in range(groups):
        shift = (iota((lanes, rows), 0) + n * per_group == iota((lanes, rows), 1)).astype(BF16)
        known = known + dot(facts_in[n], shift)
    kinds = iota((members, rows), 0).astype(F32)
    on = [(known[k : k + 1] == kinds).astype(F32) for k in range(2)]
    same = block_of((rows, 1), 0) == block_of((1, rows), 1)
    before = (same & earlier).astype(BF16)
    ranks = dot((on[0] + on[1]).astype(BF16), before)
    base = (block_of((1, rows), 1) * cap).astype(F32)
    seats = [
        known[k : k + 1] * chunk + base + jnp.sum(on[k] * ranks, 0, keepdims=True)
        for k in range(2)
    ]
    inv = (known[6:7] + known[7:8]) + known[8:9]
    table = jnp.concatenate(
        [seats[0], seats[1], known[2:3], known[3:4], known[4:5], known[5:6], inv, inv], 0
    )
    rows_t[...] = table
    cols_t[...] = jnp.transpose(
        jnp.concatenate([table, jnp.zeros((lanes - 8, rows), F32)], 0)
    )

    for off in order:
        src = lax.rem(my_g + off, groups)
        remote(
            sorted_rows.at[src], landed.at[src], s1_send.at[src], s1_recv.at[src], g=src
        ).wait_recv()
    normed[...] = (
        landed[...].reshape(rows, width).astype(F32) * cols_t[:, 6:7] * gain[...]
    ).astype(BF16)

    def pick(member):
        spots = (iota((chunk, rows), 0) + member * chunk).astype(F32)
        chosen = (spots == rows_t[0:1]) | (spots == rows_t[1:2])
        return dot(chosen.astype(F32).astype(BF16), normed[...]).astype(BF16)

    x[my_t, my_e] = pick(my_e)

    def send_rows(step, carry):
        to = lax.rem(my_e + members - step, members)
        picked[to] = pick(to)
        remote(
            picked.at[to], x.at[my_t, my_e], s2_send.at[to], s2_recv.at[my_e], e=to
        ).start()
        return carry

    lax.fori_loop(1, members, send_rows, 0)
    total[...] = jnp.zeros_like(total)
    for load in loads:
        load.wait()

    def half(ref, src, e, n):
        part = ref.shape[3] // 2
        return ref.at[src, e, :, pl.ds(n * part, part)]

    def own_to(ref, send, recv, e, n):
        return remote(
            ref.at[my_t, e], ref.at[my_t, e], send.at[n, e], recv.at[n, e],
            tp=right if n == 0 else left,
        )

    def arrived(ref, send, recv, e, n):
        src = left if n == 0 else right
        return remote(
            ref.at[src, e], ref.at[src, e], send.at[n, e], recv.at[n, e],
            tp=right if n == 0 else left,
        )

    def pass_on(ref, send, recv, e, n):
        src = left if n == 0 else right
        return remote(
            half(ref, src, e, n), half(ref, src, e, n), send.at[2 + n, e], recv.at[2 + n, e],
            tp=right if n == 0 else left,
        )

    def passed(ref, send, recv, e, n):
        return remote(
            half(ref, across, e, n), half(ref, across, e, n), send.at[2 + n, e],
            recv.at[2 + n, e], tp=right if n == 0 else left,
        )

    def stage(step, lag, body):
        @pl.when((step >= lag) & (step < members + lag))
        def _():
            body(step - lag)

    def steps(step, carry):
        def enter(i):
            e = lax.rem(my_e + i, members)

            @pl.when(i > 0)
            def _():
                remote(
                    x.at[my_t, e], x.at[my_t, e], s2_send.at[e], s2_recv.at[e], e=e
                ).wait_recv()

            for n in range(2):
                own_to(x, x_send, x_recv, e, n).start()

        def forward_x(i):
            e = lax.rem(my_e + i, members)
            for n in range(2):
                arrived(x, x_send, x_recv, e, n).wait_recv()
                pass_on(x, x_send, x_recv, e, n).start()

        def widen(i):
            e = lax.rem(my_e + i, members)
            for n in range(2):
                passed(x, x_send, x_recv, e, n).wait_recv()
            gate = jnp.zeros((chunk, ff), F32)
            up = jnp.zeros((chunk, ff), F32)
            for t in range(ways):
                piece = x[t, e]
                gate = gate + dot(piece, wg[t * width : (t + 1) * width])
                up = up + dot(piece, wu[t * width : (t + 1) * width])
            h[my_t, e] = (gate / (1.0 + jnp.exp(-gate)) * up).astype(BF16)
            for n in range(2):
                own_to(h, h_send, h_recv, e, n).start()

        def forward_h(i):
            e = lax.rem(my_e + i, members)
            for n in range(2):
                arrived(h, h_send, h_recv, e, n).wait_recv()
                pass_on(h, h_send, h_recv, e, n).start()

        def narrow(i):
            e = lax.rem(my_e + i, members)
            for n in range(2):
                passed(h, h_send, h_recv, e, n).wait_recv()
            made = jnp.zeros((chunk, width), F32)
            for t in range(ways):
                made = made + dot(h[t, e], wd[t * ff : (t + 1) * ff])

            @pl.when(i == 0)
            def _():
                back[my_e] = made.astype(BF16)

            @pl.when(i > 0)
            def _():
                result[e] = made.astype(BF16)
                remote(
                    result.at[e], back.at[my_e], r_send.at[e], r_recv.at[my_e], e=e
                ).start()

        def mix(i):
            j = lax.rem(my_e + members - i, members)

            @pl.when(i > 0)
            def _():
                remote(
                    result.at[j], back.at[j], r_send.at[j], r_recv.at[j], e=j
                ).wait_recv()

            spots = (iota((rows, chunk), 1) + j * chunk).astype(F32)
            hit = [spots == cols_t[:, k : k + 1] for k in range(2)]
            part = jnp.zeros((rows, width), F32)
            for n in range(2):
                share = jnp.where(
                    hit[0], cols_t[:, 2 + n : 3 + n], jnp.where(hit[1], cols_t[:, 4 + n : 5 + n], 0.0)
                )
                part = part + dot(share.astype(BF16), back[j])
            total[...] += part

        stage(step, 0, enter)
        stage(step, 1, forward_x)
        stage(step, 3, forward_h)
        stage(step, 2, widen)
        stage(step, 4, narrow)
        stage(step, 6, mix)
        return carry

    lax.fori_loop(0, members + 6, steps, 0)

    mixed[...] = total[...].astype(BF16).reshape(groups, per_group, width)
    f1 = []
    for off in order:
        to = lax.rem(my_g + off, groups)
        f1.append(remote(mixed.at[to], home.at[my_g], f_send.at[to], f_recv.at[my_g], g=to))
        f1[-1].start()
    home[my_g] = mixed[my_g]
    place_col = gcol[...] * per_group + rank_col.astype(jnp.int32)
    unsort = (iota((rows, rows), 1) == place_col).astype(BF16)

    for copy in q1 + s1 + m1:
        copy.wait_send()

    def drain(step, carry):
        e = lax.rem(my_e + members - step, members)
        remote(
            picked.at[e], x.at[my_t, my_e], s2_send.at[e], s2_recv.at[my_e], e=e
        ).wait_send()
        remote(
            result.at[e], back.at[my_e], r_send.at[e], r_recv.at[my_e], e=e
        ).wait_send()
        return carry

    lax.fori_loop(1, members, drain, 0)

    def drain_ways(e, carry):
        for n in range(2):
            own_to(x, x_send, x_recv, e, n).wait_send()
            pass_on(x, x_send, x_recv, e, n).wait_send()
            own_to(h, h_send, h_recv, e, n).wait_send()
            pass_on(h, h_send, h_recv, e, n).wait_send()
        return carry

    lax.fori_loop(0, members, drain_ways, 0)

    for off in order:
        src = lax.rem(my_g + off, groups)
        remote(mixed.at[src], home.at[src], f_send.at[src], f_recv.at[src], g=src).wait_recv()
    for copy in f1:
        copy.wait_send()
    out[...] = dot(unsort, home[...].reshape(rows, width)).astype(BF16)


def body(
    tokens,
    group_choice,
    expert_choice,
    group_weight,
    expert_weight,
    norm_gain,
    w_gate,
    w_up,
    w_down,
):
    rows, width = tokens.shape
    groups, members, ways = lax.axis_size("g"), lax.axis_size("e"), lax.axis_size("tp")
    per_group = rows // groups
    mean_load = 2 * per_group // members
    cap = mean_load + min(mean_load // 2, per_group - mean_load)
    chunk = groups * cap
    ff = w_gate.shape[2]
    gain = lax.dynamic_slice_in_dim(norm_gain, lax.axis_index("tp") * width, width, 0)
    dma = pltpu.SemaphoreType.DMA
    vmem = pl.BlockSpec(memory_space=pltpu.VMEM)
    hbm = pl.BlockSpec(memory_space=pl.ANY)
    return pl.pallas_call(
        functools.partial(kernel, groups, members, ways, per_group, cap),
        out_shape=jax.ShapeDtypeStruct((rows, width), BF16),
        in_specs=[vmem] * 7 + [hbm] * 3,
        out_specs=vmem,
        scratch_shapes=[
            pltpu.VMEM((ways * width, ff), BF16),
            pltpu.VMEM((ways * width, ff), BF16),
            pltpu.VMEM((ways * ff, width), BF16),
            pltpu.VMEM((ways, 8, rows), F32),
            pltpu.VMEM((groups, per_group, width), BF16),
            pltpu.VMEM((groups, 16, 128), BF16),
            pltpu.VMEM((groups, per_group, width), BF16),
            pltpu.VMEM((groups, 16, 128), BF16),
            pltpu.VMEM((rows, width), BF16),
            pltpu.VMEM((8, rows), F32),
            pltpu.VMEM((rows, 128), F32),
            pltpu.VMEM((members, chunk, width), BF16),
            pltpu.VMEM((ways, members, chunk, width), BF16),
            pltpu.VMEM((ways, members, chunk, ff), BF16),
            pltpu.VMEM((members, chunk, width), BF16),
            pltpu.VMEM((members, chunk, width), BF16),
            pltpu.VMEM((rows, width), F32),
            pltpu.VMEM((groups, per_group, width), BF16),
            pltpu.VMEM((groups, per_group, width), BF16),
            dma((3,)),
            dma((ways,)), dma((ways,)),
            dma((groups,)), dma((groups,)),
            dma((groups,)), dma((groups,)),
            dma((members,)), dma((members,)),
            dma((4, members)), dma((4, members)),
            dma((4, members)), dma((4, members)),
            dma((members,)), dma((members,)),
            dma((groups,)), dma((groups,)),
        ],
        compiler_params=pltpu.CompilerParams(
            collective_id=0, has_side_effects=True, vmem_limit_bytes=48 * 1024 * 1024
        ),
        name="expert_layer",
    )(
        tokens,
        group_choice[None, :],
        group_choice[:, None],
        expert_choice.T,
        group_weight[None, :],
        expert_weight.T,
        gain[None, :],
        w_gate[0],
        w_up[0],
        w_down[0],
    )


def solution(mesh):
    members = GROUP_SIZE
    split = Mesh(
        mesh.devices.reshape(
            mesh.shape["grp"], mesh.shape["ep"] // members, members, mesh.shape["tp"]
        ),
        ("grp", "g", "e", "tp"),
    )
    placed = (
        P(GRP_EP, "tp"),
        P(GRP_EP),
        P(GRP_EP, None),
        P(GRP_EP),
        P(GRP_EP, None),
        P(),
        P(EP, None, "tp"),
        P(EP, None, "tp"),
        P(EP, None, "tp"),
    )
    return jax.shard_map(
        body, mesh=split, in_specs=placed, out_specs=P(GRP_EP, "tp"), check_vma=False
    )
```

time: 405 us -> 220 us (0.54); the launches traced: 398 us -> 220 us
  Pallas kernels: 0 us -> 212 us
  waiting for transfers between devices: 166 us -> 0 us
  blocking collectives: 125 us -> 0 us
  starting transfers between devices: 63.2 us -> 0 us
  matrix products: 16.3 us -> 0 us
  between operations: 13.6 us -> 0.03 us
  other arithmetic: 11 us -> 0 us
  local copies, waits for them, and re-layouts: 3.1 us -> 7.56 us
    pallas_call x0 -> x1, Pallas kernels: none -> 212 us  [body(): pl.pallas_call(functools.partial(kernel, groups, members, ways, per_group...]
    all_to_all x2 -> x0, blocking collectives: 116 us -> none  [the longest x1 62.9 us: body(): lax.all_to_all(mixed.astype(jnp.bfloat16).reshape(groups, per_group, widt...]
    all_gather x2 -> x0, waiting for transfers between devices: 103 us -> none  [the longest x1 51.9 us: body(): hidden = lax.all_gather(hidden, 'tp', axis=1, tiled=True)]
    all_to_all x3 -> x0, starting transfers between devices: 63.1 us -> none  [the longest x1 43.2 us: body(): lax.all_to_all(facts.reshape(groups, per_group, 4), 'g', 0, 0, tiled=True)]
    all_to_all x3 -> x0, waiting for transfers between devices: 63 us -> none  [the longest x1 28.4 us: body(): lax.all_to_all(result.reshape(members, groups * capacity, width), 'e', 0,...]
    dot_general x9 -> x0, matrix products: 16.3 us -> none  [the longest x1 4.07 us: body(): jnp.dot(hidden, w_down[0], preferred_element_type=jnp.float32)]
    all_gather x1 -> x0, blocking collectives: 8.79 us -> none  [body(): squares = lax.all_gather(jnp.sum(values * values, -1), 'tp', axis=0)]
    unnamed x11 -> x17, local copies, waits for them, and re-layouts: 0.79 us -> 6.68 us
  transfers between devices with their start and end apart: 5 -> 0, of which waited for: 5 -> 0; matrix products, arithmetic and copies ran while one was open for 3% -> 0% of each run, Pallas kernels for 0% -> 0%
where the time goes in v2:
time: 220 us
  Pallas kernels  212 us (96%)
  local copies, waits for them, and re-layouts  7.56 us (3%)
    pallas_call x1, Pallas kernels, body(): pl.pallas_call(functools.partial(kernel, groups, members, ways, per_group...  212 us
    unnamed x17, local copies, waits for them, and re-layouts  6.68 us

profile of v2, /device:TPU:41, one launch (start us, length us, event | category | flops | bytes accessed | tf_op | source)
XLA Modules:
  0.0 220.0 jit_solution(9011108886018846172)
XLA Ops:
  0.0 0.0 copy-start.7
  0.0 0.7 copy-done.7
  0.7 0.0 copy-start.6
  0.7 0.8 dynamic_slice.3
  1.5 0.0 copy-done.6
  1.5 0.0 copy-start.4
  1.5 0.0 copy-start.5
  1.5 0.1 broadcast_in_dim.16.gcol
  1.6 0.6 copy-done.4
  2.2 0.0 copy-done.5
  2.2 0.0 copy-start
  2.2 1.2 copy-done
  3.4 0.0 copy-start.1
  3.4 1.2 copy-done.1
  4.6 0.0 copy-start.2
  4.6 1.2 copy-done.2
  5.8 0.0 copy-start.3
  5.8 1.0 copy-done.3
  6.8 212.4 %expert_layer.1 = bf16[384,512]{1,0:T(8,128)(2,1)S(1)} custom-call(bf16[384,512]{1,0:T(8,128)(2,1)S(1)} %copy-done.3, s32[1,384]{1,0:T(1,128)S(1)} %broadcast_in_dim.12.grow, s32[384,1]{1,0:T(8,128)S(1)} %broadcast_in_dim.16.gcol, s32[2,384]{1,0:T(2,128)S(1)} %bitcast.10, f32[1,384]{1,0:T(1,128)S(1)} %broadcast_in_dim.14.gw, f32[2,384]{1,0:T(2,128)S(1)} %bitcast.11, ...), custom_call_target="tpu_custom_call" | custom-call | tf_op jit(solution)/shard_map/expert_layer/pallas_call | solution.py:389
  219.2 0.7 copy.12
  (2 shorter events, 0.0 us)
Async XLA Ops:
  0.0 0.7 copy-start.7
  0.7 0.8 copy-start.6
  1.5 0.7 copy-start.4
  1.5 0.7 copy-start.5
  2.2 1.2 copy-start
  3.4 1.2 copy-start.1
  4.6 1.2 copy-start.2
  5.8 1.0 copy-start.3

commit v3 on v1

v3 whole, which is shorter than its diff:
```python
import functools

import jax
import jax.numpy as jnp
from jax import lax
from jax.experimental import pallas as pl
from jax.experimental.pallas import tpu as pltpu
from jax.sharding import Mesh
from jax.sharding import PartitionSpec as P

GRP_EP = ("grp", "g", "e")
EP = ("g", "e")
GROUP_SIZE = 8
MESH = pl.DeviceIdType.MESH
F32 = jnp.float32
BF16 = jnp.bfloat16


def dot(a, b):
    return jnp.dot(a, b, preferred_element_type=F32)


def iota(shape, dim):
    return lax.broadcasted_iota(jnp.int32, shape, dim)


def pieces(x, count):
    parts = []
    for _ in range(count):
        part = x.astype(BF16)
        parts.append(part)
        x = x - part.astype(F32)
    return parts


def remote(src, dst, send, recv, **where):
    return pltpu.make_async_remote_copy(
        src_ref=src, dst_ref=dst, send_sem=send, recv_sem=recv,
        device_id=where, device_id_type=MESH,
    )


LAGS = (0, 2, 4, 6, 8, 11)
LEAD_AT = 5
SENDS = ((1, 7, 2, 6), (3, 5, 4))
PHASES = 2


def kernel(
    groups, members, ways, per_group, cap,
    tok_hbm, grow, crow, gw, ew, gain, wg_hbm, wu_hbm, wd_hbm,
    out,
    tok, wg, wu, wd, sq, sorted_rows, facts, landed, facts_in, normed, rows_t, cols_t,
    picked, x, h, result, back, total, mixed, home,
    w_sem, q_send, q_recv, s1_send, s1_recv, m_send, m_recv, s2_send, s2_recv,
    x_send, x_recv, h_send, h_recv, r_send, r_recv, f_send, f_recv,
):
    my_g, my_e, my_t = lax.axis_index("g"), lax.axis_index("e"), lax.axis_index("tp")
    right, left = lax.rem(my_t + 1, ways), lax.rem(my_t + ways - 1, ways)
    across = lax.rem(my_t + 2, ways)
    rows, width = tok.shape
    slots = groups // PHASES
    some = rows // PHASES
    chunk = slots * cap
    chunks = PHASES * members
    ff = wg.shape[1]
    lanes = 128
    wide = 2 * lanes

    tok_load = pltpu.make_async_copy(tok_hbm, tok, w_sem.at[3])
    tok_load.start()
    loads = [
        pltpu.make_async_copy(src, dst, w_sem.at[n])
        for n, (src, dst) in enumerate(((wg_hbm, wg), (wu_hbm, wu), (wd_hbm, wd)))
    ]
    for load in loads:
        load.start()

    barrier = pltpu.get_barrier_semaphore()

    def greet(**where):
        pl.semaphore_signal(barrier, inc=1, device_id=where, device_id_type=MESH)

    near = members // 2
    my_part = my_e // near

    def leader_of(k):
        if k == near:
            return lax.rem(my_e + near, members)
        return (k // near) * near + lax.rem(my_e + k, near)

    def slot_there(k):
        if k == near:
            return groups - 2
        return 2 * (min(k, groups - k) - 1) + my_part

    def source_of(slot):
        if slot == groups - 2:
            return near, lax.rem(my_e + near, members)
        away = slot // 2 + 1
        k = away + my_part * (groups - 2 * away)
        return k, lax.rem(my_e + groups - k, near) + (slot % 2) * near

    def back_by(k):
        return lax.rem(my_g + groups - k, groups)

    for k in range(1, groups):
        greet(g=lax.rem(my_g + k, groups), e=leader_of(k))
    for slot in range(groups - 1):
        k, e = source_of(slot)
        greet(g=back_by(k), e=e)
    for off in range(1, members):
        greet(e=lax.rem(my_e + off, members))
    for off in range(1, ways):
        greet(tp=lax.rem(my_t + off, ways))

    earlier = iota((rows, rows), 0) < iota((rows, rows), 1)
    marks = (grow[...] == iota((groups, rows), 0)).astype(F32)
    rank_row = jnp.sum(dot(marks.astype(BF16), earlier.astype(BF16)) * marks, 0, keepdims=True)
    place_row = grow[...] * per_group + rank_row.astype(jnp.int32)
    sort = (iota((rows, rows), 0) == place_row).astype(BF16)
    two = jnp.concatenate(
        [place_row.astype(F32), grow[...] * lanes + rank_row, jnp.zeros((lanes - 2, rows), F32)], 0
    )
    place_cols = jnp.transpose(two)
    place_col, place_wide = place_cols[:, 0:1], place_cols[:, 1:2]
    tok_load.wait()
    sorted_rows[...] = dot(sort, tok[...]).astype(BF16).reshape(groups, per_group, width)
    values = tok[...].astype(F32)
    squares = jnp.sum(values * values, -1, keepdims=True)
    squares = jnp.transpose(jnp.broadcast_to(squares, (rows, lanes)))
    sq[my_t] = squares[:8]

    with jax.named_scope("barrier_wait"):
        pl.semaphore_wait(barrier, 2 * groups + members + ways - 4)

    def rows_out(k):
        to = lax.rem(my_g + k, groups)
        slot = slot_there(k)
        return remote(
            sorted_rows.at[to], landed.at[slot], s1_send.at[k], s1_recv.at[slot],
            g=to, e=leader_of(k),
        )

    def rows_in(slot):
        k, e = source_of(slot)
        return remote(
            sorted_rows.at[slot], landed.at[slot], s1_send.at[slot], s1_recv.at[slot],
            g=back_by(k), e=e,
        )

    def facts_out(k):
        to = lax.rem(my_g + k, groups)
        slot = slot_there(k)
        return remote(
            facts.at[to], facts_in.at[slot], m_send.at[k], m_recv.at[slot],
            g=to, e=leader_of(k),
        )

    def facts_to_me(slot):
        k, e = source_of(slot)
        return remote(
            facts.at[slot], facts_in.at[slot], m_send.at[slot], m_recv.at[slot],
            g=back_by(k), e=e,
        )

    def home_out(slot):
        k, e = source_of(slot)
        return remote(
            mixed.at[slot], home.at[my_g], f_send.at[slot], f_recv.at[k], g=back_by(k), e=e
        )

    def home_in(k):
        src = lax.rem(my_g + k, groups)
        return remote(
            mixed.at[k], home.at[src], f_send.at[k], f_recv.at[k], g=src, e=leader_of(k)
        )

    q1 = []
    for off in range(1, ways):
        to = lax.rem(my_t + off, ways)
        q1.append(remote(sq.at[my_t], sq.at[my_t], q_send.at[to], q_recv.at[my_t], tp=to))
        q1[-1].start()
    for k in SENDS[0]:
        rows_out(k).start()
    landed[groups - 1] = sorted_rows[my_g]

    spread = (iota((rows, groups * lanes), 1).astype(F32) == place_wide).astype(BF16)
    with jax.named_scope("sq_wait"):
        for off in range(1, ways):
            src = lax.rem(my_t + off, ways)
            remote(sq.at[src], sq.at[src], q_send.at[src], q_recv.at[src], tp=src).wait_recv()
    model_width = width * ways
    all_squares = jnp.sum(sq[...], 0)[:1]
    inv_rms = lax.rsqrt(all_squares / model_width + 1e-06)
    weights = ew[...]
    mixing = gw[...] * weights / jnp.sum(weights, 0, keepdims=True)
    choice = crow[...].astype(F32)
    fields = [choice[0:1], choice[1:2]]
    for k in range(2):
        fields += [p.astype(F32) for p in pieces(mixing[k : k + 1], 2)]
    fields += [p.astype(F32) for p in pieces(inv_rms, 3)]
    fields.append(jnp.zeros((16 - len(fields), rows), F32))
    fields = jnp.concatenate(fields, 0).astype(BF16)
    spread_fields = dot(fields, spread).astype(BF16)
    for n in range(groups):
        facts[n] = spread_fields[:, n * lanes : (n + 1) * lanes]
    for k in SENDS[0] + SENDS[1]:
        facts_out(k).start()
    facts_in[groups - 1] = facts[my_g]
    for load in loads:
        load.wait()

    def block_of(shape, dim):
        spot = iota(shape, dim)
        block = jnp.zeros(shape, jnp.int32)
        for n in range(1, slots):
            block = block + (spot >= n * per_group).astype(jnp.int32)
        return block

    def lead(phase):
        first = phase * slots
        with jax.named_scope("facts_wait"):
            for slot in range(first, min(first + slots, groups - 1)):
                facts_to_me(slot).wait_recv()
        known = jnp.zeros((16, wide), F32)
        for n in range(slots):
            shift = (iota((lanes, wide), 0) + n * per_group == iota((lanes, wide), 1)).astype(BF16)
            known = known + dot(facts_in[first + n], shift)
        kinds = iota((members, wide), 0).astype(F32)
        on = [(known[k : k + 1] == kinds).astype(F32) for k in range(2)]
        same = block_of((wide, 1), 0) == block_of((1, wide), 1)
        before = (same & (iota((wide, wide), 0) < iota((wide, wide), 1))).astype(BF16)
        ranks = dot((on[0] + on[1]).astype(BF16), before)
        base = (block_of((1, wide), 1) * cap).astype(F32)
        seats = [
            known[k : k + 1] * chunk + base + jnp.sum(on[k] * ranks, 0, keepdims=True)
            for k in range(2)
        ]
        inv = (known[6:7] + known[7:8]) + known[8:9]
        table = jnp.concatenate(
            [seats[0], seats[1], known[2:3], known[3:4], known[4:5], known[5:6], inv, inv], 0
        )
        rows_t[phase] = table
        cols_t[phase] = jnp.transpose(
            jnp.concatenate([table, jnp.zeros((lanes - 8, wide), F32)], 0)
        )
        with jax.named_scope("landed_wait"):
            for slot in range(first, min(first + slots, groups - 1)):
                rows_in(slot).wait_recv()
        if phase == 0:
            for k in SENDS[1]:
                rows_out(k).start()
        scale = gain[:, pl.ds(pl.multiple_of(my_t * width, width), width)]
        normed[...] = (
            landed[first : first + slots].reshape(some, width).astype(F32)
            * cols_t[phase, :some, 6:7]
            * scale
        ).astype(BF16)

        def pick(member):
            spots = (iota((chunk, some), 0) + member * chunk).astype(F32)
            chosen = (spots == rows_t[phase, 0:1, :some]) | (spots == rows_t[phase, 1:2, :some])
            return dot(chosen.astype(F32).astype(BF16), normed[...]).astype(BF16)

        x[my_t, phase * members + my_e] = pick(my_e)

        def send_rows(step, carry):
            to = lax.rem(my_e + members - step, members)
            picked[phase * members + to] = pick(to)
            rows_to(phase * members + to, phase * members + my_e, to).start()
            return carry

        lax.fori_loop(1, members, send_rows, 0)

    def rows_to(there, here, to):
        return remote(
            picked.at[there], x.at[my_t, here], s2_send.at[there], s2_recv.at[here], e=to
        )

    def result_to(there, here, to):
        return remote(
            result.at[there], back.at[here], r_send.at[there], r_recv.at[here], e=to
        )

    def half(ref, src, c, n):
        part = ref.shape[3] // 2
        return ref.at[src, c, :, pl.ds(n * part, part)]

    def own_to(ref, send, recv, c, n):
        return remote(
            ref.at[my_t, c], ref.at[my_t, c], send.at[n, c], recv.at[n, c],
            tp=right if n == 0 else left,
        )

    def arrived(ref, send, recv, c, n):
        src = left if n == 0 else right
        return remote(
            ref.at[src, c], ref.at[src, c], send.at[n, c], recv.at[n, c],
            tp=right if n == 0 else left,
        )

    def pass_on(ref, send, recv, c, n):
        src = left if n == 0 else right
        return remote(
            half(ref, src, c, n), half(ref, src, c, n), send.at[2 + n, c], recv.at[2 + n, c],
            tp=right if n == 0 else left,
        )

    def passed(ref, send, recv, c, n):
        return remote(
            half(ref, across, c, n), half(ref, across, c, n), send.at[2 + n, c],
            recv.at[2 + n, c], tp=right if n == 0 else left,
        )

    def enter(i, off, phase, e, c):
        @pl.when(off > 0)
        def _():
            rows_to(c, c, e).wait_recv()

        for n in range(2):
            own_to(x, x_send, x_recv, c, n).start()

    def forward_x(i, off, phase, e, c):
        for n in range(2):
            arrived(x, x_send, x_recv, c, n).wait_recv()
            pass_on(x, x_send, x_recv, c, n).start()

    def widen(i, off, phase, e, c):
        for n in range(2):
            passed(x, x_send, x_recv, c, n).wait_recv()
        gate = jnp.zeros((chunk, ff), F32)
        up = jnp.zeros((chunk, ff), F32)
        for t in range(ways):
            piece = x[t, c]
            gate = gate + dot(piece, wg[t * width : (t + 1) * width])
            up = up + dot(piece, wu[t * width : (t + 1) * width])
        h[my_t, c] = (gate / (1.0 + jnp.exp(-gate)) * up).astype(BF16)
        for n in range(2):
            own_to(h, h_send, h_recv, c, n).start()

    def forward_h(i, off, phase, e, c):
        for n in range(2):
            arrived(h, h_send, h_recv, c, n).wait_recv()
            pass_on(h, h_send, h_recv, c, n).start()

    def narrow(i, off, phase, e, c):
        for n in range(2):
            passed(h, h_send, h_recv, c, n).wait_recv()
        made = jnp.zeros((chunk, width), F32)
        for t in range(ways):
            made = made + dot(h[t, c], wd[t * ff : (t + 1) * ff])

        @pl.when(off == 0)
        def _():
            back[c] = made.astype(BF16)

        @pl.when(off > 0)
        def _():
            result[c] = made.astype(BF16)
            result_to(c, phase * members + my_e, e).start()

    def mix(i, off, phase, e, c):
        j = lax.rem(my_e + members - off, members)
        there = phase * members + j

        @pl.when(off > 0)
        def _():
            result_to(there, there, j).wait_recv()

        spots = (iota((some, chunk), 1) + j * chunk).astype(F32)
        hit = [spots == cols_t[phase, :some, k : k + 1] for k in range(2)]
        part = jnp.zeros((some, width), F32)
        for n in range(2):
            share = jnp.where(
                hit[0],
                cols_t[phase, :some, 2 + n : 3 + n],
                jnp.where(hit[1], cols_t[phase, :some, 4 + n : 5 + n], 0.0),
            )
            part = part + dot(share.astype(BF16), back[there])

        @pl.when(off == 0)
        def _():
            total[...] = part

        @pl.when(off > 0)
        def _():
            total[...] += part

        for p in range(PHASES):
            @pl.when(i == (p + 1) * members - 1)
            def _():
                first = p * slots
                mixed[first : first + slots] = (
                    total[...].astype(BF16).reshape(slots, per_group, width)
                )
                for slot in range(first, min(first + slots, groups - 1)):
                    home_out(slot).start()

    def stage(step, lag, name, body):
        with jax.named_scope(name):
            @pl.when((step >= lag) & (step < chunks + lag))
            def _():
                i = step - lag
                phase, off = i // members, lax.rem(i, members)
                e = lax.rem(my_e + off, members)
                body(i, off, phase, e, phase * members + e)

    def steps(step, carry):
        stage(step, LAGS[0], "enter", enter)
        stage(step, LAGS[1], "forward_x", forward_x)
        stage(step, LAGS[3], "forward_h", forward_h)
        stage(step, LAGS[2], "widen", widen)
        stage(step, LAGS[4], "narrow", narrow)
        stage(step, LAGS[5], "mix", mix)

        @pl.when(step == LEAD_AT)
        def _():
            lead(1)

        return carry

    lead(0)
    lax.fori_loop(0, chunks + LAGS[5], steps, 0)
    home[my_g] = mixed[groups - 1]
    unsort = (iota((rows, rows), 1).astype(F32) == place_col).astype(BF16)

    for copy in q1:
        copy.wait_send()
    for k in range(1, groups):
        rows_out(k).wait_send()
        facts_out(k).wait_send()

    def drain(step, carry):
        phase, off = step // members, lax.rem(step, members)

        @pl.when(off > 0)
        def _():
            e = lax.rem(my_e + off, members)
            rows_to(phase * members + e, phase * members + my_e, e).wait_send()
            result_to(phase * members + e, phase * members + my_e, e).wait_send()

        for n in range(2):
            own_to(x, x_send, x_recv, step, n).wait_send()
            pass_on(x, x_send, x_recv, step, n).wait_send()
            own_to(h, h_send, h_recv, step, n).wait_send()
            pass_on(h, h_send, h_recv, step, n).wait_send()
        return carry

    lax.fori_loop(0, chunks, drain, 0)
    with jax.named_scope("home_wait"):
        for k in range(1, groups):
            home_in(k).wait_recv()
    for slot in range(groups - 1):
        home_out(slot).wait_send()
    out[...] = dot(unsort, home[...].reshape(rows, width)).astype(BF16)


def body(
    tokens,
    group_choice,
    expert_choice,
    group_weight,
    expert_weight,
    norm_gain,
    w_gate,
    w_up,
    w_down,
):
    rows, width = tokens.shape
    groups, members, ways = lax.axis_size("g"), lax.axis_size("e"), lax.axis_size("tp")
    per_group = rows // groups
    mean_load = 2 * per_group // members
    cap = mean_load + min(mean_load // 2, per_group - mean_load)
    chunk = groups // PHASES * cap
    chunks = PHASES * members
    some = rows // PHASES
    ff = w_gate.shape[2]
    dma = pltpu.SemaphoreType.DMA
    vmem = pl.BlockSpec(memory_space=pltpu.VMEM)
    hbm = pl.BlockSpec(memory_space=pltpu.HBM)
    return pl.pallas_call(
        functools.partial(kernel, groups, members, ways, per_group, cap),
        out_shape=jax.ShapeDtypeStruct((rows, width), BF16),
        in_specs=[hbm] + [vmem] * 5 + [hbm] * 3,
        out_specs=vmem,
        scratch_shapes=[
            pltpu.VMEM((rows, width), BF16),
            pltpu.VMEM((ways * width, ff), BF16),
            pltpu.VMEM((ways * width, ff), BF16),
            pltpu.VMEM((ways * ff, width), BF16),
            pltpu.VMEM((ways, 8, rows), F32),
            pltpu.VMEM((groups, per_group, width), BF16),
            pltpu.VMEM((groups, 16, 128), BF16),
            pltpu.VMEM((groups, per_group, width), BF16),
            pltpu.VMEM((groups, 16, 128), BF16),
            pltpu.VMEM((some, width), BF16),
            pltpu.VMEM((PHASES, 8, 256), F32),
            pltpu.VMEM((PHASES, 256, 128), F32),
            pltpu.VMEM((chunks, chunk, width), BF16),
            pltpu.VMEM((ways, chunks, chunk, width), BF16),
            pltpu.VMEM((ways, chunks, chunk, ff), BF16),
            pltpu.VMEM((chunks, chunk, width), BF16),
            pltpu.VMEM((chunks, chunk, width), BF16),
            pltpu.VMEM((some, width), F32),
            pltpu.VMEM((groups, per_group, width), BF16),
            pltpu.VMEM((groups, per_group, width), BF16),
            dma((4,)),
            dma((ways,)), dma((ways,)),
            dma((groups,)), dma((groups,)),
            dma((groups,)), dma((groups,)),
            dma((chunks,)), dma((chunks,)),
            dma((4, chunks)), dma((4, chunks)),
            dma((4, chunks)), dma((4, chunks)),
            dma((chunks,)), dma((chunks,)),
            dma((groups,)), dma((groups,)),
        ],
        compiler_params=pltpu.CompilerParams(
            collective_id=0, has_side_effects=True, vmem_limit_bytes=62 * 1024 * 1024
        ),
        name="expert_layer",
    )(
        tokens,
        group_choice[None, :],
        expert_choice.T,
        group_weight[None, :],
        expert_weight.T,
        norm_gain[None, :],
        w_gate[0],
        w_up[0],
        w_down[0],
    )


def solution(mesh):
    members = GROUP_SIZE
    split = Mesh(
        mesh.devices.reshape(
            mesh.shape["grp"], mesh.shape["ep"] // members, members, mesh.shape["tp"]
        ),
        ("grp", "g", "e", "tp"),
    )
    placed = (
        P(GRP_EP, "tp"),
        P(GRP_EP),
        P(GRP_EP, None),
        P(GRP_EP),
        P(GRP_EP, None),
        P(),
        P(EP, None, "tp"),
        P(EP, None, "tp"),
        P(EP, None, "tp"),
    )
    return jax.shard_map(
        body, mesh=split, in_specs=placed, out_specs=P(GRP_EP, "tp"), check_vma=False
    )
```

time: 405 us -> 203 us (0.50)
  the two profiles are of different devices: /device:TPU:41 before, /device:TPU:97 now
where the time goes in v3:
time: 203 us
  Pallas kernels  199 us (98%)
  local copies, waits for them, and re-layouts  3.72 us (2%)
    pallas_call x1, Pallas kernels, body(): pl.pallas_call(functools.partial(kernel, groups, members, ways, per_group...  199 us

profile of v3, /device:TPU:97, one launch (start us, length us, event | category | flops | bytes accessed | tf_op | source)
XLA Modules:
  0.0 202.9 jit_solution(13715956138726253724)
XLA Ops:
  0.0 0.0 copy-start
  0.0 0.7 copy-done
  0.7 0.0 copy-start.1
  0.7 0.6 broadcast_in_dim.9.grow
  1.2 0.1 copy-done.1
  1.4 0.6 broadcast_in_dim.10.gw
  2.0 199.1 %expert_layer.1 = bf16[384,512]{1,0:T(8,128)(2,1)} custom-call(bf16[384,512]{1,0:T(8,128)(2,1)} %tok_hbm.1, s32[1,384]{1,0:T(1,128)} %broadcast_in_dim.9.grow, s32[2,384]{1,0:T(2,128)} %bitcast.10, f32[1,384]{1,0:T(1,128)} %broadcast_in_dim.10.gw, f32[2,384]{1,0:T(2,128)} %bitcast.11, f32[1,2048]{1,0:T(1,128)} %bitcast.9, bf16[2048,256]{1,0:T(8,128)(2,1)} %bitcast.6, ...), custom_call_target="tpu_custom_call" | custom-call | tf_op jit(solution)/shard_map/expert_layer/pallas_call | solution.py:482
  201.1 1.8 copy.11
Async XLA Ops:
  0.0 0.7 copy-start
  0.7 0.7 copy-start.1

commit v4 on v3

--- a/solution.py
+++ b/solution.py
@@ -40,10 +40,11 @@
     )
 
 
-LAGS = (0, 2, 4, 6, 8, 11)
-LEAD_AT = 5
-SENDS = ((1, 7, 2, 6), (3, 5, 4))
-PHASES = 2
+LAGS = (0, 2, 4, 7, 9, 13)
+AWAY = (1, 4, 3, 2)
+PHASES = 4
+LEAD_AT = (6, 14, 22)
+UPFRONT = 2
 
 
 def kernel(
@@ -65,7 +66,7 @@
     chunks = PHASES * members
     ff = wg.shape[1]
     lanes = 128
-    wide = 2 * lanes
+    wide = -(-some // lanes) * lanes
 
     tok_load = pltpu.make_async_copy(tok_hbm, tok, w_sem.at[3])
     tok_load.start()
@@ -82,6 +83,17 @@
         pl.semaphore_signal(barrier, inc=1, device_id=where, device_id_type=MESH)
 
     near = members // 2
+    home_slot = 2 * AWAY.index(near) + 1
+    per_phase = len(AWAY) // PHASES
+    sends = [
+        sum([(a,) if a == near else (a, groups - a) for a in AWAY[n : n + per_phase]], ())
+        for n in range(0, len(AWAY), per_phase)
+    ]
+
+    def slots_of(phase):
+        every = range(groups // PHASES * phase, groups // PHASES * (phase + 1))
+        return [slot for slot in every if slot != home_slot]
+
     my_part = my_e // near
 
     def leader_of(k):
@@ -91,13 +103,13 @@
 
     def slot_there(k):
         if k == near:
-            return groups - 2
-        return 2 * (min(k, groups - k) - 1) + my_part
+            return home_slot - 1
+        return 2 * AWAY.index(min(k, groups - k)) + my_part
 
     def source_of(slot):
-        if slot == groups - 2:
+        if slot == home_slot - 1:
             return near, lax.rem(my_e + near, members)
-        away = slot // 2 + 1
+        away = AWAY[slot // 2]
         k = away + my_part * (groups - 2 * away)
         return k, lax.rem(my_e + groups - k, near) + (slot % 2) * near
 
@@ -106,9 +118,10 @@
 
     for k in range(1, groups):
         greet(g=lax.rem(my_g + k, groups), e=leader_of(k))
-    for slot in range(groups - 1):
-        k, e = source_of(slot)
-        greet(g=back_by(k), e=e)
+    for phase in range(PHASES):
+        for slot in slots_of(phase):
+            k, e = source_of(slot)
+            greet(g=back_by(k), e=e)
     for off in range(1, members):
         greet(e=lax.rem(my_e + off, members))
     for off in range(1, ways):
@@ -181,9 +194,9 @@
         to = lax.rem(my_t + off, ways)
         q1.append(remote(sq.at[my_t], sq.at[my_t], q_send.at[to], q_recv.at[my_t], tp=to))
         q1[-1].start()
-    for k in SENDS[0]:
+    for k in sum(sends[:UPFRONT], ()):
         rows_out(k).start()
-    landed[groups - 1] = sorted_rows[my_g]
+    landed[home_slot] = sorted_rows[my_g]
 
     spread = (iota((rows, groups * lanes), 1).astype(F32) == place_wide).astype(BF16)
     with jax.named_scope("sq_wait"):
@@ -205,9 +218,9 @@
     spread_fields = dot(fields, spread).astype(BF16)
     for n in range(groups):
         facts[n] = spread_fields[:, n * lanes : (n + 1) * lanes]
-    for k in SENDS[0] + SENDS[1]:
+    for k in sum(sends, ()):
         facts_out(k).start()
-    facts_in[groups - 1] = facts[my_g]
+    facts_in[home_slot] = facts[my_g]
     for load in loads:
         load.wait()
 
@@ -221,7 +234,7 @@
     def lead(phase):
         first = phase * slots
         with jax.named_scope("facts_wait"):
-            for slot in range(first, min(first + slots, groups - 1)):
+            for slot in slots_of(phase):
                 facts_to_me(slot).wait_recv()
         known = jnp.zeros((16, wide), F32)
         for n in range(slots):
@@ -246,11 +259,8 @@
             jnp.concatenate([table, jnp.zeros((lanes - 8, wide), F32)], 0)
         )
         with jax.named_scope("landed_wait"):
-            for slot in range(first, min(first + slots, groups - 1)):
+            for slot in slots_of(phase):
                 rows_in(slot).wait_recv()
-        if phase == 0:
-            for k in SENDS[1]:
-                rows_out(k).start()
         scale = gain[:, pl.ds(pl.multiple_of(my_t * width, width), width)]
         normed[...] = (
             landed[first : first + slots].reshape(some, width).astype(F32)
@@ -272,6 +282,9 @@
             return carry
 
         lax.fori_loop(1, members, send_rows, 0)
+        if phase + UPFRONT < PHASES:
+            for k in sends[phase + UPFRONT]:
+                rows_out(k).start()
 
     def rows_to(there, here, to):
         return remote(
@@ -394,7 +407,7 @@
                 mixed[first : first + slots] = (
                     total[...].astype(BF16).reshape(slots, per_group, width)
                 )
-                for slot in range(first, min(first + slots, groups - 1)):
+                for slot in slots_of(p):
                     home_out(slot).start()
 
     def stage(step, lag, name, body):
@@ -414,15 +427,16 @@
         stage(step, LAGS[4], "narrow", narrow)
         stage(step, LAGS[5], "mix", mix)
 
-        @pl.when(step == LEAD_AT)
-        def _():
-            lead(1)
+        for p in range(1, PHASES):
+            @pl.when(step == LEAD_AT[p - 1])
+            def _():
+                lead(p)
 
         return carry
 
     lead(0)
     lax.fori_loop(0, chunks + LAGS[5], steps, 0)
-    home[my_g] = mixed[groups - 1]
+    home[my_g] = mixed[home_slot]
     unsort = (iota((rows, rows), 1).astype(F32) == place_col).astype(BF16)
 
     for copy in q1:
@@ -451,8 +465,9 @@
     with jax.named_scope("home_wait"):
         for k in range(1, groups):
             home_in(k).wait_recv()
-    for slot in range(groups - 1):
-        home_out(slot).wait_send()
+    for phase in range(PHASES):
+        for slot in slots_of(phase):
+            home_out(slot).wait_send()
     out[...] = dot(unsort, home[...].reshape(rows, width)).astype(BF16)
 
 
@@ -475,6 +490,7 @@
     chunk = groups // PHASES * cap
     chunks = PHASES * members
     some = rows // PHASES
+    wide = -(-some // 128) * 128
     ff = w_gate.shape[2]
     dma = pltpu.SemaphoreType.DMA
     vmem = pl.BlockSpec(memory_space=pltpu.VMEM)
@@ -495,8 +511,8 @@
             pltpu.VMEM((groups, per_group, width), BF16),
             pltpu.VMEM((groups, 16, 128), BF16),
             pltpu.VMEM((some, width), BF16),
-            pltpu.VMEM((PHASES, 8, 256), F32),
-            pltpu.VMEM((PHASES, 256, 128), F32),
+            pltpu.VMEM((PHASES, 8, wide), F32),
+            pltpu.VMEM((PHASES, wide, 128), F32),
             pltpu.VMEM((chunks, chunk, width), BF16),
             pltpu.VMEM((ways, chunks, chunk, width), BF16),
             pltpu.VMEM((ways, chunks, chunk, ff), BF16),

time: 203 us -> 190 us (0.936)
  the two profiles are of different devices: /device:TPU:97 before, /device:TPU:41 now
where the time goes in v4:
time: 190 us; the launch traced here: 189 us
  Pallas kernels  186 us (98%)
  local copies, waits for them, and re-layouts  3.72 us (2%)
    pallas_call x1, Pallas kernels, body(): pl.pallas_call(functools.partial(kernel, groups, members, ways, per_group...  186 us

profile of v4, /device:TPU:41, one launch (start us, length us, event | category | flops | bytes accessed | tf_op | source)
XLA Modules:
  0.0 189.3 jit_solution(14375830663145947946)
XLA Ops:
  0.0 0.0 copy-start
  0.0 0.7 copy-done
  0.7 0.0 copy-start.1
  0.7 0.6 broadcast_in_dim.9.grow
  1.2 0.1 copy-done.1
  1.4 0.6 broadcast_in_dim.10.gw
  2.0 185.6 %expert_layer.1 = bf16[384,512]{1,0:T(8,128)(2,1)} custom-call(bf16[384,512]{1,0:T(8,128)(2,1)} %tok_hbm.1, s32[1,384]{1,0:T(1,128)} %broadcast_in_dim.9.grow, s32[2,384]{1,0:T(2,128)} %bitcast.10, f32[1,384]{1,0:T(1,128)} %broadcast_in_dim.10.gw, f32[2,384]{1,0:T(2,128)} %bitcast.11, f32[1,2048]{1,0:T(1,128)} %bitcast.9, bf16[2048,256]{1,0:T(8,128)(2,1)} %bitcast.6, ...), custom_call_target="tpu_custom_call" | custom-call | tf_op jit(solution)/shard_map/expert_layer/pallas_call | solution.py:498
  187.5 1.8 copy.11
Async XLA Ops:
  0.0 0.7 copy-start
  0.7 0.7 copy-start.1

commit v5 on v4

--- a/solution.py
+++ b/solution.py
@@ -41,7 +41,7 @@
 
 
 LAGS = (0, 2, 4, 7, 9, 13)
-AWAY = (1, 4, 3, 2)
+AWAY = (2, 4, 3, 1)
 PHASES = 4
 LEAD_AT = (6, 14, 22)
 UPFRONT = 2

time: 190 us -> 195 us (1.026)
  Pallas kernels: 186 us -> 191 us
    pallas_call x1, Pallas kernels: 186 us -> 191 us  [body(): pl.pallas_call(functools.partial(kernel, groups, members, ways, per_group...]
where the time goes in v5:
time: 195 us
  Pallas kernels  191 us (98%)
  local copies, waits for them, and re-layouts  3.72 us (2%)
    pallas_call x1, Pallas kernels, body(): pl.pallas_call(functools.partial(kernel, groups, members, ways, per_group...  191 us

profile of v5, /device:TPU:41, one launch (start us, length us, event | category | flops | bytes accessed | tf_op | source)
XLA Modules:
  0.0 194.9 jit_solution(16231504037704554833)
XLA Ops:
  0.0 0.0 copy-start
  0.0 0.7 copy-done
  0.7 0.0 copy-start.1
  0.7 0.6 broadcast_in_dim.9.grow
  1.2 0.1 copy-done.1
  1.4 0.6 broadcast_in_dim.10.gw
  2.0 191.2 %expert_layer.1 = bf16[384,512]{1,0:T(8,128)(2,1)} custom-call(bf16[384,512]{1,0:T(8,128)(2,1)} %tok_hbm.1, s32[1,384]{1,0:T(1,128)} %broadcast_in_dim.9.grow, s32[2,384]{1,0:T(2,128)} %bitcast.10, f32[1,384]{1,0:T(1,128)} %broadcast_in_dim.10.gw, f32[2,384]{1,0:T(2,128)} %bitcast.11, f32[1,2048]{1,0:T(1,128)} %bitcast.9, bf16[2048,256]{1,0:T(8,128)(2,1)} %bitcast.6, ...), custom_call_target="tpu_custom_call" | custom-call | tf_op jit(solution)/shard_map/expert_layer/pallas_call | solution.py:498
  193.2 1.8 copy.11
Async XLA Ops:
  0.0 0.7 copy-start
  0.7 0.7 copy-start.1
